TPU v7x, 32 devices: a whole 2x2x4 slice. The times are simulated.
32 devices in a mesh: sp: 8 (over z, x), dp: 4 (over y, core).
Axes of the slice: x: 2, y: 2, z: 4, core: 2. Of those that a mesh axis runs over, the one named last changes fastest.
Arguments:
- queries: bfloat16 [4, 1024, 2048], P('dp', 'sp'), may hold values from -6 to 6
- keys: bfloat16 [4, 1024, 2048], P('dp', 'sp'), may hold values from -6 to 6
- values: bfloat16 [4, 1024, 2048], P('dp', 'sp'), may hold values from -6 to 6
- gate_totals: float32 [4, 1024, 32], P('dp', 'sp'), may hold values from -1024 to 0, as said below
- w_out: bfloat16 [2048, 2048], P(None, 'dp'), may hold values from -1 to 1
Outputs:
- mixed: bfloat16 [4, 1024, 2048], P('dp', 'sp')
Inputs may be any that keep to these rules, and one draw needn't show every extreme that they name: `gate_totals`: never rising along a sequence.
All inputs are finite; a program needn't handle non-finite values.
Results may differ from a plain program's by a relative error of at most 0.0053.
Values may be sent and summed in bfloat16 or wider, within the bound.
A program may use at most 64 MiB of HBM per device.

v0:
```python
import jax
import jax.numpy as jnp
from jax import lax
from jax.sharding import PartitionSpec as P

HEAD_DIM = 64


def attend(queries, key_rows, value_rows, totals):
    length = queries.shape[0]
    block_rows = min(length, 512)
    pieces = []
    for begin_row in range(0, length, block_rows):
        end_row = begin_row + block_rows
        scaled = queries[begin_row:end_row] * jnp.bfloat16(HEAD_DIM ** (-0.5))
        scores = jnp.einsum(
            "qhd,khd->hqk", scaled, key_rows[:end_row], preferred_element_type=jnp.float32
        )
        causal = jnp.arange(end_row)[None, :] <= (begin_row + jnp.arange(block_rows))[:, None]
        scores = jnp.where(
            causal[None],
            scores
            + jnp.transpose(totals[begin_row:end_row])[:, :, None]
            - jnp.transpose(totals[:end_row])[:, None, :],
            -jnp.inf,
        )
        biggest = jnp.max(scores, axis=-1, keepdims=True)
        expo = jnp.exp(scores - biggest)
        summed = jnp.sum(expo, axis=-1)
        weights = expo.astype(jnp.bfloat16)
        output = jnp.einsum(
            "hqk,khd->qhd", weights, value_rows[:end_row], preferred_element_type=jnp.float32
        )
        output = output / jnp.transpose(summed)[:, :, None]
        pieces.append(output.astype(jnp.bfloat16))
    return jnp.concatenate(pieces, axis=0).reshape(length, -1)


def local(queries, keys, values, gate_totals, w_out):
    moved = (
        lax.all_to_all(queries, "sp", split_axis=2, concat_axis=1, tiled=True),
        lax.all_to_all(keys, "sp", split_axis=2, concat_axis=1, tiled=True),
        lax.all_to_all(values, "sp", split_axis=2, concat_axis=1, tiled=True),
    )
    totals = lax.all_to_all(gate_totals, "sp", split_axis=2, concat_axis=1, tiled=True)
    held, length = (moved[0].shape[0], moved[0].shape[1])
    query_heads, key_heads, value_heads = [
        part_array[0].reshape(length, -1, HEAD_DIM) for part_array in moved
    ]
    outputs = [attend(query_heads, key_heads, value_heads, totals[0])]
    attended = jnp.stack(outputs, axis=0)
    local_rows = lax.all_to_all(attended, "sp", split_axis=1, concat_axis=2, tiled=True)
    flat_rows = local_rows.reshape(-1, local_rows.shape[2])
    mixed = jnp.dot(
        flat_rows,
        lax.all_gather(w_out, "dp", axis=1, tiled=True),
        preferred_element_type=jnp.float32,
    )
    return mixed.astype(jnp.bfloat16).reshape(local_rows.shape[0], local_rows.shape[1], -1)


def solution(mesh):
    placed = (
        P("dp", "sp", None),
        P("dp", "sp", None),
        P("dp", "sp", None),
        P("dp", "sp", None),
        P(None, "dp"),
    )
    return jax.shard_map(
        local, mesh=mesh, in_specs=placed, out_specs=P("dp", "sp", None), check_vma=False
    )
```

profile of v0, /device:TPU:0, one launch (start us, length us, event | category | flops | bytes accessed | tf_op | source)
XLA Modules:
  0.0 138.5 jit_solution(7458643636415226542)
XLA Ops:
  6.5 0.0 all-gather.2.cloned.1.call-start
  6.5 0.7 all-gather.2.cloned.1.call-update
  7.3 7.3 %all-to-all-start.2 = ((f32[1,128,32]{1,0,2:T(1,128)}), f32[1,128,32]{1,0,2:T(1,128)S(1)}, u32[]{:S(2)}, u32[]{:S(2)}) async-start(f32[1,128,32]{1,0,2:T(1,128)} %bitcast.98), calls=%async_computation.2 | async-start | bytes 32768 | tf_op jit(solution)/shard_map/all_to_all | solution.py:45
  14.6 2.3 %copy.32 = bf16[1,128,2048]{1,0,2:T(2,128)(2,1)S(1)} copy(bf16[1,128,2048]{2,1,0:T(8,128)(2,1)} %param.6) | data formatting | bytes 1048576 | tf_op args[1]
  16.9 0.6 broadcast.36
  17.5 11.6 %reduce.2 = bf16[2048,128]{1,0:T(8,128)(2,1)S(1)} reduce(bf16[2048,1,128]{2,1,0:T(2,128)(2,1)S(1)} %bitcast.83, bf16[]{:T(256)} %broadcast.36), dimensions={1}, to_apply=%bitcast.66.reduce_sub_computation | reduce | bytes 1048578
  29.0 1.0 reshape.70
  30.0 0.0 all-to-all-done.2
  30.0 6.0 %all-to-all-start.1 = ((bf16[8,2,16384]{2,1,0:T(2,128)(2,1)}), bf16[8,2,16384]{2,1,0:T(2,128)(2,1)S(1)}, u32[]{:S(2)}, u32[]{:S(2)}) async-start(bf16[8,2,16384]{2,1,0:T(2,128)(2,1)} %reshape.70), calls=%async_computation.1 | async-start | bytes 1048576 | tf_op jit(solution)/shard_map/all_to_all | solution.py:42
  36.0 0.0 copy-done.2
  36.0 0.8 copy.35
  36.8 11.5 %reduce = bf16[2048,128]{1,0:T(8,128)(2,1)S(1)} reduce(bf16[2048,1,128]{2,1,0:T(2,128)(2,1)S(1)} %bitcast.85, bf16[]{:T(256)} %broadcast.36), dimensions={1}, to_apply=%bitcast.62.reduce_sub_computation | reduce | bytes 1048578
  48.3 0.9 reshape.66
  49.2 0.8 all-to-all-done.1
  50.0 5.2 %all-to-all-start.3 = ((bf16[8,2,16384]{2,1,0:T(2,128)(2,1)}), bf16[8,2,16384]{2,1,0:T(2,128)(2,1)S(1)}, u32[]{:S(2)}, u32[]{:S(2)}) async-start(bf16[8,2,16384]{2,1,0:T(2,128)(2,1)} %reshape.66), calls=%async_computation.3 | async-start | bytes 1048576 | tf_op jit(solution)/shard_map/all_to_all | solution.py:43
  55.2 0.0 copy-done.3
  55.2 0.8 copy.30
  56.0 11.5 %reduce.1 = bf16[2048,128]{1,0:T(8,128)(2,1)S(1)} reduce(bf16[2048,1,128]{2,1,0:T(2,128)(2,1)S(1)} %bitcast.86, bf16[]{:T(256)} %broadcast.36), dimensions={1}, to_apply=%bitcast.64.reduce_sub_computation | reduce | bytes 1048578
  67.5 1.0 reshape.68
  68.5 0.1 all-to-all-done.3
  68.6 5.9 %all-to-all-start = ((bf16[8,2,16384]{2,1,0:T(2,128)(2,1)}), bf16[8,2,16384]{2,1,0:T(2,128)(2,1)S(1)}, u32[]{:S(2)}, u32[]{:S(2)}) async-start(bf16[8,2,16384]{2,1,0:T(2,128)(2,1)} %reshape.68), calls=%async_computation | async-start | bytes 1048576 | tf_op jit(solution)/shard_map/all_to_all | solution.py:41
  74.5 0.1 iota_compare_fusion.1
  74.5 0.4 iota_compare_fusion
  74.9 0.5 reshape.71
  75.5 0.1 copy.46
  75.5 0.3 copy.39
  75.9 0.7 slice.45
  76.6 0.5 reshape.67
  77.2 0.1 copy.44
  77.2 0.3 copy.40
  77.6 0.7 slice.43
  78.3 8.9 %all-to-all-done = bf16[8,2,16384]{2,1,0:T(2,128)(2,1)S(1)} async-done(((bf16[8,2,16384]{2,1,0:T(2,128)(2,1)}), bf16[8,2,16384]{2,1,0:T(2,128)(2,1)S(1)}, u32[]{:S(2)}, u32[]{:S(2)}) %all-to-all-start) | async-done | bytes 524320 | tf_op jit(solution)/shard_map/all_to_all | solution.py:41
  87.2 0.5 reshape.69
  87.8 0.0 copy-start
  87.8 0.0 copy-start.1
  87.8 0.1 copy.45
  87.9 0.2 copy.38
  88.1 0.8 mul.15
  89.0 1.0 reshape_squeeze.7
  90.0 0.2 reshape_squeeze.8
  90.2 0.2 copy.31
  90.4 0.1 mul.13
  90.5 0.2 copy.33
  90.7 0.1 slice.35
  90.9 0.2 copy.36
  91.1 0.1 slice.39
  91.2 1.2 fusion.8
  92.3 1.2 fusion.6
  93.6 0.0 copy-start.4
  93.6 1.4 %fusion.22 = bf16[512,4,64]{0,2,1:T(8,128)(2,1)S(1)} fusion(bf16[512,4,64]{0,2,1:T(8,128)(2,1)S(1)} %slice.39, f32[4,512,512]{1,2,0:T(8,128)S(1)} %get-tuple-element.12, f32[4,512]{1,0:T(4,128)S(1)} %get-tuple-element.11, f32[4,512]{1,0:T(4,128)S(1)} %get-tuple-element.7, pred[512,512]{0,1:T(8,128)(4,1)S(1)} %iota_compare_fusion.1, f32[512,4]{0,1:T(4,128)S(1)} %bitcast.100), kind=kOutput, calls=%fused_computation.21 | convolution fusion | flops 139722752 | bytes 5005312 | tf_op jit(solution)/shard_map/hqk,khd->qhd/dot_general | solution.py:31
  95.1 0.0 copy-done.4
  95.1 2.2 %fusion.2 = (f32[4,512]{1,0:T(4,128)S(1)}, f32[4,512,1024]{2,1,0:T(8,128)S(1)}) fusion(f32[4,1024]{1,0:T(4,128)S(1)} %bitcast.95, f32[4,512]{1,0:T(4,128)S(1)} %get-tuple-element.8, pred[512,1024]{1,0:T(8,128)(4,1)S(1)} %iota_compare_fusion, bf16[512,4,64]{0,2,1:T(8,128)(2,1)S(1)} %copy-done.5, bf16[1024,4,64]{0,2,1:T(8,128)(2,1)S(1)} %copy-done.4), kind=kOutput, calls=%fused_computation.4 | convolution fusion | flops 276822016 | bytes 9732096 | tf_op jit(solution)/shard_map/qhd,khd->hqk/dot_general | solution.py:16
  97.3 2.8 %fusion = f32[4,512]{1,0:T(4,128)S(1)} fusion(f32[4,512,1024]{2,1,0:T(8,128)S(1)} %get-tuple-element.10, f32[4,512]{1,0:T(4,128)S(1)} %get-tuple-element.9, f32[4,1024]{1,0:T(4,128)S(1)} %bitcast.96, f32[4,512]{1,0:T(4,128)S(1)} %get-tuple-element.8, pred[512,1024]{1,0:T(8,128)(4,1)S(1)} %iota_compare_fusion), kind=kLoop, calls=%fused_computation.2 | loop fusion | flops 10483712 | bytes 8953856 | tf_op jit(solution)/shard_map/reduce_sum | solution.py:29
  100.1 2.8 %fusion.28 = bf16[512,4,64]{0,2,1:T(8,128)(2,1)S(1)} fusion(bf16[1024,4,64]{0,2,1:T(8,128)(2,1)S(1)} %reshape_squeeze.8, f32[4,512,1024]{2,1,0:T(8,128)S(1)} %get-tuple-element.10, f32[4,512]{1,0:T(4,128)S(1)} %get-tuple-element.9, f32[4,1024]{1,0:T(4,128)S(1)} %bitcast.97, f32[4,512]{1,0:T(4,128)S(1)} %get-tuple-element.8, ...), kind=kOutput, calls=%fused_computation.23 | convolution fusion | flops 279183360 | bytes 9740288 | tf_op jit(solution)/shard_map/hqk,khd->qhd/dot_general | solution.py:31
  102.9 0.1 pad_maximum_fusion
  103.0 1.1 copy.41
  104.1 3.8 %reduce.3 = bf16[1024,256]{1,0:T(8,128)(2,1)S(1)} reduce(bf16[1024,1,256]{2,1,0:T(2,128)(2,1)S(1)} %bitcast.84, bf16[]{:T(256)} %broadcast.36), dimensions={1}, to_apply=%bitcast.68.reduce_sub_computation | reduce | bytes 1048578
  107.9 0.1 reshape.72
  108.0 17.2 %all_to_all.75 = bf16[8,2,16384]{2,1,0:T(2,128)(2,1)S(1)} all-to-all(bf16[8,2,16384]{2,1,0:T(2,128)(2,1)S(1)} %reshape.72), channel_id=1, replica_groups=mesh['sp'=8,'dp'=4] {'sp'}, dimensions={0} | all-to-all | bytes 1048576 | tf_op jit(solution)/shard_map/all_to_all | solution.py:52
  125.2 0.5 reshape.73
  125.8 0.1 copy.47
  125.9 0.3 copy.42
  126.1 0.0 all-gather.2.cloned.1.call-done
  126.2 5.5 %fusion.9 = bf16[1,128,2048]{2,1,0:T(8,128)(2,1)} fusion(bf16[128,2048]{0,1:T(8,128)(2,1)S(1)} %bitcast.78, bf16[2048,2048]{1,0:T(8,128)(2,1)} %all-gather.2.cloned.1.call-done), kind=kOutput, calls=%fused_computation.13 | convolution fusion | flops 1074003968 | bytes 9437184 | tf_op jit(solution)/shard_map/dot_general | solution.py:54
  (9 shorter events, 0.1 us)
Async XLA Ops:
  6.5 29.5 %copy-start.2 = (bf16[1,128,2048]{2,1,0:T(8,128)(2,1)S(1)}, bf16[1,128,2048]{2,1,0:T(8,128)(2,1)}, u32[]{:S(2)}) copy-start(bf16[1,128,2048]{2,1,0:T(8,128)(2,1)} %param.7) | copy-start | bytes 1572868
  6.5 119.6 %all-gather.2.cloned.1.call-start = ((), (), s32[]{:S(2)}) async-start(), calls=%async_computation.5 | async-start | bytes 10485760 | tf_op jit(solution)/shard_map/all_gather | solution.py:56
  7.3 22.8 %all-to-all-start.2 = ((f32[1,128,32]{1,0,2:T(1,128)}), f32[1,128,32]{1,0,2:T(1,128)S(1)}, u32[]{:S(2)}, u32[]{:S(2)}) async-start(f32[1,128,32]{1,0,2:T(1,128)} %bitcast.98), calls=%async_computation.2 | async-start | bytes 32768 | tf_op jit(solution)/shard_map/all_to_all | solution.py:45
  17.5 37.7 %copy-start.3 = (bf16[1,128,2048]{2,1,0:T(8,128)(2,1)S(1)}, bf16[1,128,2048]{2,1,0:T(8,128)(2,1)}, u32[]{:S(2)}) copy-start(bf16[1,128,2048]{2,1,0:T(8,128)(2,1)} %param.5) | copy-start | bytes 1572868
  30.0 20.0 %all-to-all-start.1 = ((bf16[8,2,16384]{2,1,0:T(2,128)(2,1)}), bf16[8,2,16384]{2,1,0:T(2,128)(2,1)S(1)}, u32[]{:S(2)}, u32[]{:S(2)}) async-start(bf16[8,2,16384]{2,1,0:T(2,128)(2,1)} %reshape.70), calls=%async_computation.1 | async-start | bytes 1048576 | tf_op jit(solution)/shard_map/all_to_all | solution.py:42
  50.0 18.6 %all-to-all-start.3 = ((bf16[8,2,16384]{2,1,0:T(2,128)(2,1)}), bf16[8,2,16384]{2,1,0:T(2,128)(2,1)S(1)}, u32[]{:S(2)}, u32[]{:S(2)}) async-start(bf16[8,2,16384]{2,1,0:T(2,128)(2,1)} %reshape.66), calls=%async_computation.3 | async-start | bytes 1048576 | tf_op jit(solution)/shard_map/all_to_all | solution.py:43
  68.6 18.7 %all-to-all-start = ((bf16[8,2,16384]{2,1,0:T(2,128)(2,1)}), bf16[8,2,16384]{2,1,0:T(2,128)(2,1)S(1)}, u32[]{:S(2)}, u32[]{:S(2)}) async-start(bf16[8,2,16384]{2,1,0:T(2,128)(2,1)} %reshape.68), calls=%async_computation | async-start | bytes 1048576 | tf_op jit(solution)/shard_map/all_to_all | solution.py:41
  87.8 2.7 %copy-start = (bf16[1,4,128,256]{2,3,1,0:T(8,128)(2,1)S(1)}, bf16[1,4,128,256]{2,3,1,0:T(8,128)(2,1)}, u32[]{:S(2)}) copy-start(bf16[1,4,128,256]{2,3,1,0:T(8,128)(2,1)} %slice.45) | copy-start | bytes 786436
  87.8 3.1 %copy-start.1 = (bf16[1,4,128,256]{2,3,1,0:T(8,128)(2,1)S(1)}, bf16[1,4,128,256]{2,3,1,0:T(8,128)(2,1)}, u32[]{:S(2)}) copy-start(bf16[1,4,128,256]{2,3,1,0:T(8,128)(2,1)} %slice.43) | copy-start | bytes 786436
  93.6 1.5 %copy-start.4 = (bf16[1024,4,64]{0,2,1:T(8,128)(2,1)S(1)}, bf16[1024,4,64]{0,2,1:T(8,128)(2,1)}, u32[]{:S(2)}) copy-start(bf16[1024,4,64]{0,2,1:T(8,128)(2,1)} %reshape_squeeze.7) | copy-start | bytes 1572868
  93.6 1.5 %copy-start.5 = (bf16[512,4,64]{0,2,1:T(8,128)(2,1)S(1)}, bf16[512,4,64]{0,2,1:T(8,128)(2,1)}, u32[]{:S(2)}) copy-start(bf16[512,4,64]{0,2,1:T(8,128)(2,1)} %mul.15) | copy-start | bytes 786436
Sparse Core Ops, SparseCore 0:
  8.9 60.9 all-gather.1
where the time goes:
time: 139 us; the launch traced here: 138 us
  other arithmetic  43 us (31%)
  starting transfers between devices  24.4 us (18%)
  blocking collectives  17.2 us (12%)
  local copies, waits for them, and re-layouts  16.5 us (12%)
  between operations  13.7 us (10%)
  matrix products  13.1 us (9%)
  waiting for transfers between devices  10.5 us (8%)
    unnamed x4, other arithmetic  38.4 us
    all_to_all x1, blocking collectives, local(): lax.all_to_all(attended, 'sp', split_axis=1, concat_axis=2, tiled=True)  17.2 us
    unnamed x28, local copies, waits for them, and re-layouts  9.83 us
    all_to_all x1, waiting for transfers between devices, local(): lax.all_to_all(queries, 'sp', split_axis=2, concat_axis=1, tiled=True)  8.91 us
    all_to_all x1, starting transfers between devices, local(): lax.all_to_all(gate_totals, 'sp', split_axis=2, concat_axis=1, tiled=True)  7.29 us
    all_to_all x1, starting transfers between devices, local(): lax.all_to_all(keys, 'sp', split_axis=2, concat_axis=1, tiled=True)  6 us
    all_to_all x1, starting transfers between devices, local(): lax.all_to_all(queries, 'sp', split_axis=2, concat_axis=1, tiled=True)  5.88 us
    dot_general x1, matrix products, local(): jnp.dot(flat_rows, lax.all_gather(w_out, 'dp', axis=1, tiled=True), prefe...  5.46 us
  transfers between devices with their start and end apart: 5, of which 3 were waited for; matrix products, arithmetic and copies ran while one was open for 48% of the time, Pallas kernels for 0%

commit v1 on v0

--- a/solution.py
+++ b/solution.py
@@ -4,6 +4,13 @@
 from jax.sharding import PartitionSpec as P
 
 HEAD_DIM = 64
+
+
+def trade_parts(array, axis, split, join):
+    devices = lax.axis_size(axis)
+    shards = jnp.stack(jnp.split(array, devices, axis=split), axis=0)
+    shards = lax.all_to_all(shards, axis, split_axis=0, concat_axis=0)
+    return jnp.concatenate(shards, axis=join)
 
 
 def attend(queries, key_rows, value_rows, totals):
@@ -49,7 +56,7 @@
     ]
     outputs = [attend(query_heads, key_heads, value_heads, totals[0])]
     attended = jnp.stack(outputs, axis=0)
-    local_rows = lax.all_to_all(attended, "sp", split_axis=1, concat_axis=2, tiled=True)
+    local_rows = trade_parts(attended, "sp", 1, 2)
     flat_rows = local_rows.reshape(-1, local_rows.shape[2])
     mixed = jnp.dot(
         flat_rows,

time: 139 us -> 133 us (0.957)
  other arithmetic: 43 us -> 39.2 us
  local copies, waits for them, and re-layouts: 16.5 us -> 14.7 us
    unnamed x4 -> x3, other arithmetic: 38.4 us -> 34.6 us
    unnamed x28 -> x32, local copies, waits for them, and re-layouts: 9.83 us -> 9.31 us
  transfers between devices with their start and end apart: 5 -> 5, of which waited for: 3 -> 3; matrix products, arithmetic and copies ran while one was open for 48% -> 46% of each run, Pallas kernels for 0% -> 0%
where the time goes in v1:
time: 133 us
  other arithmetic  39.2 us (29%)
  starting transfers between devices  24.4 us (18%)
  blocking collectives  17.2 us (13%)
  local copies, waits for them, and re-layouts  14.7 us (11%)
  between operations  13.7 us (10%)
  matrix products  13.1 us (10%)
  waiting for transfers between devices  10.5 us (8%)
    unnamed x3, other arithmetic  34.6 us
    all_to_all x1, blocking collectives, trade_parts(): shards = lax.all_to_all(shards, axis, split_axis=0, concat_axis=0)  17.2 us
    unnamed x32, local copies, waits for them, and re-layouts  9.31 us
    all_to_all x1, waiting for transfers between devices, local(): lax.all_to_all(queries, 'sp', split_axis=2, concat_axis=1, tiled=True)  8.91 us
    all_to_all x1, starting transfers between devices, local(): lax.all_to_all(gate_totals, 'sp', split_axis=2, concat_axis=1, tiled=True)  7.29 us
    all_to_all x1, starting transfers between devices, local(): lax.all_to_all(keys, 'sp', split_axis=2, concat_axis=1, tiled=True)  6 us
    all_to_all x1, starting transfers between devices, local(): lax.all_to_all(queries, 'sp', split_axis=2, concat_axis=1, tiled=True)  5.88 us
    dot_general x1, matrix products, local(): jnp.dot(flat_rows, lax.all_gather(w_out, 'dp', axis=1, tiled=True), prefe...  5.46 us
  transfers between devices with their start and end apart: 5, of which 3 were waited for; matrix products, arithmetic and copies ran while one was open for 46% of the time, Pallas kernels for 0%

profile of v1, /device:TPU:0, one launch (start us, length us, event | category | flops | bytes accessed | tf_op | source)
XLA Modules:
  0.0 132.8 jit_solution(10239288332971865691)
XLA Ops:
  6.5 0.0 copy-start.2
  6.5 0.0 all-gather.2.cloned.1.call-start
  6.5 0.7 all-gather.2.cloned.1.call-update
  7.3 7.3 %all-to-all-start.2 = ((f32[1,128,32]{1,0,2:T(1,128)}), f32[1,128,32]{1,0,2:T(1,128)S(1)}, u32[]{:S(2)}, u32[]{:S(2)}) async-start(f32[1,128,32]{1,0,2:T(1,128)} %bitcast.131), calls=%async_computation.2 | async-start | bytes 32768 | tf_op jit(solution)/shard_map/all_to_all | solution.py:52
  14.6 2.3 %copy.20 = bf16[1,128,2048]{1,0,2:T(2,128)(2,1)S(1)} copy(bf16[1,128,2048]{2,1,0:T(8,128)(2,1)} %param.6) | data formatting | bytes 1048576 | tf_op args[1]
  16.9 0.6 broadcast.36
  17.5 0.0 copy-start.3
  17.5 11.6 %reduce.2 = bf16[2048,128]{1,0:T(8,128)(2,1)S(1)} reduce(bf16[2048,1,128]{2,1,0:T(2,128)(2,1)S(1)} %bitcast.111, bf16[]{:T(256)} %broadcast.36), dimensions={1}, to_apply=%bitcast.97.reduce_sub_computation | reduce | bytes 1048578
  29.0 1.0 reshape.69
  30.0 0.0 all-to-all-done.2
  30.0 6.0 %all-to-all-start.1 = ((bf16[8,2,16384]{2,1,0:T(2,128)(2,1)}), bf16[8,2,16384]{2,1,0:T(2,128)(2,1)S(1)}, u32[]{:S(2)}, u32[]{:S(2)}) async-start(bf16[8,2,16384]{2,1,0:T(2,128)(2,1)} %reshape.69), calls=%async_computation.1 | async-start | bytes 1048576 | tf_op jit(solution)/shard_map/all_to_all | solution.py:49
  36.0 0.0 copy-done.2
  36.0 0.8 copy.23
  36.8 11.5 %reduce = bf16[2048,128]{1,0:T(8,128)(2,1)S(1)} reduce(bf16[2048,1,128]{2,1,0:T(2,128)(2,1)S(1)} %bitcast.113, bf16[]{:T(256)} %broadcast.36), dimensions={1}, to_apply=%bitcast.93.reduce_sub_computation | reduce | bytes 1048578
  48.3 0.9 reshape.65
  49.2 0.8 all-to-all-done.1
  50.0 5.2 %all-to-all-start.3 = ((bf16[8,2,16384]{2,1,0:T(2,128)(2,1)}), bf16[8,2,16384]{2,1,0:T(2,128)(2,1)S(1)}, u32[]{:S(2)}, u32[]{:S(2)}) async-start(bf16[8,2,16384]{2,1,0:T(2,128)(2,1)} %reshape.65), calls=%async_computation.3 | async-start | bytes 1048576 | tf_op jit(solution)/shard_map/all_to_all | solution.py:50
  55.2 0.0 copy-done.3
  55.2 0.8 copy.18
  56.0 11.5 %reduce.1 = bf16[2048,128]{1,0:T(8,128)(2,1)S(1)} reduce(bf16[2048,1,128]{2,1,0:T(2,128)(2,1)S(1)} %bitcast.112, bf16[]{:T(256)} %broadcast.36), dimensions={1}, to_apply=%bitcast.95.reduce_sub_computation | reduce | bytes 1048578
  67.5 1.0 reshape.67
  68.5 0.1 all-to-all-done.3
  68.6 5.9 %all-to-all-start = ((bf16[8,2,16384]{2,1,0:T(2,128)(2,1)}), bf16[8,2,16384]{2,1,0:T(2,128)(2,1)S(1)}, u32[]{:S(2)}, u32[]{:S(2)}) async-start(bf16[8,2,16384]{2,1,0:T(2,128)(2,1)} %reshape.67), calls=%async_computation | async-start | bytes 1048576 | tf_op jit(solution)/shard_map/all_to_all | solution.py:48
  74.4 0.1 iota_compare_fusion.1
  74.5 0.4 iota_compare_fusion
  74.9 0.5 reshape.70
  75.5 0.1 copy.32
  75.5 0.3 copy.27
  75.9 0.7 slice.45
  76.6 0.5 reshape.66
  77.2 0.1 copy.30
  77.2 0.3 copy.28
  77.6 0.7 slice.43
  78.3 8.9 %all-to-all-done = bf16[8,2,16384]{2,1,0:T(2,128)(2,1)S(1)} async-done(((bf16[8,2,16384]{2,1,0:T(2,128)(2,1)}), bf16[8,2,16384]{2,1,0:T(2,128)(2,1)S(1)}, u32[]{:S(2)}, u32[]{:S(2)}) %all-to-all-start) | async-done | bytes 524320 | tf_op jit(solution)/shard_map/all_to_all | solution.py:48
  87.2 0.5 reshape.68
  87.8 0.0 copy-start
  87.8 0.0 copy-start.1
  87.8 0.1 copy.31
  87.9 0.2 copy.26
  88.1 0.8 mul.15
  89.0 1.0 reshape_squeeze.7
  90.0 0.2 reshape_squeeze.8
  90.2 0.2 copy.19
  90.4 0.1 mul.13
  90.5 0.0 copy-done
  90.6 0.2 copy.21
  90.8 0.1 slice.35
  90.9 0.0 copy-done.1
  90.9 0.2 copy.24
  91.1 0.1 slice.39
  91.2 1.2 fusion.8
  92.4 1.2 fusion.6
  93.6 0.0 copy-start.4
  93.6 0.0 copy-start.5
  93.6 1.4 %fusion.22 = bf16[512,4,64]{0,2,1:T(8,128)(2,1)S(1)} fusion(bf16[512,4,64]{0,2,1:T(8,128)(2,1)S(1)} %slice.39, f32[4,512,512]{1,2,0:T(8,128)S(1)} %get-tuple-element.12, f32[4,512]{1,0:T(4,128)S(1)} %get-tuple-element.11, f32[4,512]{1,0:T(4,128)S(1)} %get-tuple-element.7, pred[512,512]{0,1:T(8,128)(4,1)S(1)} %iota_compare_fusion.1, f32[512,4]{0,1:T(4,128)S(1)} %bitcast.133), kind=kOutput, calls=%fused_computation.21 | convolution fusion | flops 139722752 | bytes 5005312 | tf_op jit(solution)/shard_map/hqk,khd->qhd/dot_general | solution.py:38
  95.1 0.0 copy-done.4
  95.1 0.0 copy-done.5
  95.1 2.2 %fusion.2 = (f32[4,512]{1,0:T(4,128)S(1)}, f32[4,512,1024]{2,1,0:T(8,128)S(1)}) fusion(f32[4,1024]{1,0:T(4,128)S(1)} %bitcast.128, f32[4,512]{1,0:T(4,128)S(1)} %get-tuple-element.8, pred[512,1024]{1,0:T(8,128)(4,1)S(1)} %iota_compare_fusion, bf16[512,4,64]{0,2,1:T(8,128)(2,1)S(1)} %copy-done.5, bf16[1024,4,64]{0,2,1:T(8,128)(2,1)S(1)} %copy-done.4), kind=kOutput, calls=%fused_computation.4 | convolution fusion | flops 276822016 | bytes 9732096 | tf_op jit(solution)/shard_map/qhd,khd->hqk/dot_general | solution.py:23
  97.3 2.8 %fusion = f32[4,512]{1,0:T(4,128)S(1)} fusion(f32[4,512,1024]{2,1,0:T(8,128)S(1)} %get-tuple-element.10, f32[4,512]{1,0:T(4,128)S(1)} %get-tuple-element.9, f32[4,1024]{1,0:T(4,128)S(1)} %bitcast.129, f32[4,512]{1,0:T(4,128)S(1)} %get-tuple-element.8, pred[512,1024]{1,0:T(8,128)(4,1)S(1)} %iota_compare_fusion), kind=kLoop, calls=%fused_computation.2 | loop fusion | flops 10483712 | bytes 8953856 | tf_op jit(solution)/shard_map/reduce_sum | solution.py:36
  100.2 2.8 %fusion.28 = bf16[512,4,64]{0,2,1:T(8,128)(2,1)S(1)} fusion(bf16[1024,4,64]{0,2,1:T(8,128)(2,1)S(1)} %reshape_squeeze.8, f32[4,512,1024]{2,1,0:T(8,128)S(1)} %get-tuple-element.10, f32[4,512]{1,0:T(4,128)S(1)} %get-tuple-element.9, f32[4,1024]{1,0:T(4,128)S(1)} %bitcast.130, f32[4,512]{1,0:T(4,128)S(1)} %get-tuple-element.8, ...), kind=kOutput, calls=%fused_computation.23 | convolution fusion | flops 279183360 | bytes 9740288 | tf_op jit(solution)/shard_map/hqk,khd->qhd/dot_general | solution.py:38
  103.0 0.1 pad_maximum_fusion
  103.3 17.2 %all_to_all.65 = bf16[8,1,128,256]{2,3,1,0:T(8,128)(2,1)S(1)} all-to-all(bf16[8,1,128,256]{2,3,1,0:T(8,128)(2,1)S(1)} %fusion.31), channel_id=1, replica_groups=mesh['sp'=8,'dp'=4] {'sp'}, dimensions={0} | all-to-all | bytes 1048576 | tf_op jit(solution)/shard_map/all_to_all | solution.py:12
  120.5 0.0 all-gather.2.cloned.1.call-done
  120.5 5.5 %fusion.9 = bf16[1,128,2048]{2,1,0:T(8,128)(2,1)} fusion(bf16[128,2048]{0,1:T(8,128)(2,1)S(1)} %bitcast.107, bf16[2048,2048]{1,0:T(8,128)(2,1)} %all-gather.2.cloned.1.call-done), kind=kOutput, calls=%fused_computation.13 | convolution fusion | flops 1074003968 | bytes 9437184 | tf_op jit(solution)/shard_map/dot_general | solution.py:61
  (11 shorter events, 0.3 us)
Async XLA Ops:
  6.5 29.5 %copy-start.2 = (bf16[1,128,2048]{2,1,0:T(8,128)(2,1)S(1)}, bf16[1,128,2048]{2,1,0:T(8,128)(2,1)}, u32[]{:S(2)}) copy-start(bf16[1,128,2048]{2,1,0:T(8,128)(2,1)} %param.7) | copy-start | bytes 1572868
  6.5 114.0 %all-gather.2.cloned.1.call-start = ((), (), s32[]{:S(2)}) async-start(), calls=%async_computation.5 | async-start | bytes 10485760 | tf_op jit(solution)/shard_map/all_gather | solution.py:63
  7.3 22.8 %all-to-all-start.2 = ((f32[1,128,32]{1,0,2:T(1,128)}), f32[1,128,32]{1,0,2:T(1,128)S(1)}, u32[]{:S(2)}, u32[]{:S(2)}) async-start(f32[1,128,32]{1,0,2:T(1,128)} %bitcast.131), calls=%async_computation.2 | async-start | bytes 32768 | tf_op jit(solution)/shard_map/all_to_all | solution.py:52
  17.5 37.7 %copy-start.3 = (bf16[1,128,2048]{2,1,0:T(8,128)(2,1)S(1)}, bf16[1,128,2048]{2,1,0:T(8,128)(2,1)}, u32[]{:S(2)}) copy-start(bf16[1,128,2048]{2,1,0:T(8,128)(2,1)} %param.5) | copy-start | bytes 1572868
  30.0 20.0 %all-to-all-start.1 = ((bf16[8,2,16384]{2,1,0:T(2,128)(2,1)}), bf16[8,2,16384]{2,1,0:T(2,128)(2,1)S(1)}, u32[]{:S(2)}, u32[]{:S(2)}) async-start(bf16[8,2,16384]{2,1,0:T(2,128)(2,1)} %reshape.69), calls=%async_computation.1 | async-start | bytes 1048576 | tf_op jit(solution)/shard_map/all_to_all | solution.py:49
  50.0 18.6 %all-to-all-start.3 = ((bf16[8,2,16384]{2,1,0:T(2,128)(2,1)}), bf16[8,2,16384]{2,1,0:T(2,128)(2,1)S(1)}, u32[]{:S(2)}, u32[]{:S(2)}) async-start(bf16[8,2,16384]{2,1,0:T(2,128)(2,1)} %reshape.65), calls=%async_computation.3 | async-start | bytes 1048576 | tf_op jit(solution)/shard_map/all_to_all | solution.py:50
  68.6 18.7 %all-to-all-start = ((bf16[8,2,16384]{2,1,0:T(2,128)(2,1)}), bf16[8,2,16384]{2,1,0:T(2,128)(2,1)S(1)}, u32[]{:S(2)}, u32[]{:S(2)}) async-start(bf16[8,2,16384]{2,1,0:T(2,128)(2,1)} %reshape.67), calls=%async_computation | async-start | bytes 1048576 | tf_op jit(solution)/shard_map/all_to_all | solution.py:48
  87.8 2.8 %copy-start = (bf16[1,4,128,256]{2,3,1,0:T(8,128)(2,1)S(1)}, bf16[1,4,128,256]{2,3,1,0:T(8,128)(2,1)}, u32[]{:S(2)}) copy-start(bf16[1,4,128,256]{2,3,1,0:T(8,128)(2,1)} %slice.45) | copy-start | bytes 786436
  87.8 3.1 %copy-start.1 = (bf16[1,4,128,256]{2,3,1,0:T(8,128)(2,1)S(1)}, bf16[1,4,128,256]{2,3,1,0:T(8,128)(2,1)}, u32[]{:S(2)}) copy-start(bf16[1,4,128,256]{2,3,1,0:T(8,128)(2,1)} %slice.43) | copy-start | bytes 786436
  93.6 1.5 %copy-start.4 = (bf16[1024,4,64]{0,2,1:T(8,128)(2,1)S(1)}, bf16[1024,4,64]{0,2,1:T(8,128)(2,1)}, u32[]{:S(2)}) copy-start(bf16[1024,4,64]{0,2,1:T(8,128)(2,1)} %reshape_squeeze.7) | copy-start | bytes 1572868
  93.6 1.5 %copy-start.5 = (bf16[512,4,64]{0,2,1:T(8,128)(2,1)S(1)}, bf16[512,4,64]{0,2,1:T(8,128)(2,1)}, u32[]{:S(2)}) copy-start(bf16[512,4,64]{0,2,1:T(8,128)(2,1)} %mul.15) | copy-start | bytes 786436
Sparse Core Ops, SparseCore 0:
  8.9 60.9 all-gather.1
